TPU v7x, 32 devices: a whole 2x2x4 slice. The times are simulated.
32 devices in a mesh: ep: 8 (over z, core), tp: 4 (over y, x).
Axes of the slice: x: 2, y: 2, z: 4, core: 2. Of those that a mesh axis runs over, the one named last changes fastest.
Arguments:
- query_rows: bfloat16 [6144, 1024], P('ep', 'tp'), may hold values from -600 to 600
- key_rows: bfloat16 [6144, 1024], P('ep', 'tp'), may hold values from -6 to 6
- value_rows: bfloat16 [6144, 1024], P('ep', 'tp'), may hold values from -6 to 6
- cum_gate: float32 [16, 6144], P('tp'), may hold values from -615 to 0, as said below
- out_weight: bfloat16 [1024, 2048], P(None, 'tp'), may hold values from -0.1875 to 0.1875
- moe_input: bfloat16 [1536, 2048], P('ep'), may hold values from -6 to 6
- moe_gain: float32 [2048], replicated, may hold values from 0.1 to 1.9
- routes: int32 [1536, 3], P('ep'), may hold values from 0 to 31, all different within a row; in each aligned block of 192 rows (0 to 191, 192 to 383, ...) at most 36 rows name the same one
- route_weight: float32 [1536, 3], P('ep'), may hold values from 0.2 to 1.5
- expert_gate: bfloat16 [32, 2048, 512], P('ep', None, 'tp'), may hold values from -0.125 to 0.125
- expert_up: bfloat16 [32, 2048, 512], P('ep', None, 'tp'), may hold values from -0.125 to 0.125
- expert_down: bfloat16 [32, 512, 2048], P('ep', None, 'tp'), may hold values from -0.25 to 0.25
- shared_gate: bfloat16 [2048, 512], P(None, 'tp'), may hold values from -0.125 to 0.125
- shared_up: bfloat16 [2048, 512], P(None, 'tp'), may hold values from -0.125 to 0.125
- shared_down: bfloat16 [512, 2048], P(None, 'tp'), may hold values from -0.25 to 0.25
Outputs:
- mixer_out: bfloat16 [6144, 2048], P('ep', 'tp')
- moe_out: bfloat16 [1536, 2048], P('ep', 'tp')
Inputs may be any that keep to these rules, and one draw needn't show every extreme that they name: Non-increasing along positions: cum_gate[h, t] is the sum of the log forget gates of head h over positions 0 to t. `routes`: the 3 experts of a token differ. In each aligned block of 192 tokens no expert is named by more than 36 tokens, a bound that some block reaches.
All inputs are finite; a program needn't handle non-finite values.
Results may differ from a plain program's by a relative error of at most 0.0068.
Values may be sent and summed in bfloat16 or wider, within the bound.
A program may use at most 64 MiB of HBM per device.

v0:
```python
import jax
import jax.numpy as jnp
from jax import lax
from jax.sharding import PartitionSpec as P

HEAD = 64
neg_fill = -1e30
norm_eps = 1e-06


def local(
    query_rows,
    key_rows,
    value_rows,
    cum_gate,
    out_weight,
    moe_input,
    moe_gain,
    routes,
    route_weight,
    expert_gate,
    expert_up,
    expert_down,
    shared_gate,
    shared_up,
    shared_down,
):
    row_count = query_rows.shape[0]
    width = query_rows.shape[1]
    local_heads = width // HEAD
    scale = HEAD ** (-0.5)
    first_row = lax.axis_index("ep") * row_count
    last_row = first_row + row_count - 1
    query_heads = query_rows.reshape(row_count, local_heads, HEAD)
    query_gate = lax.dynamic_slice_in_dim(cum_gate, first_row, row_count, 1)
    query_pos = first_row + jnp.arange(row_count, dtype=jnp.int32)
    key_value = jnp.concatenate([key_rows, value_rows], axis=1)
    initial = (
        jnp.full((local_heads, row_count), neg_fill, jnp.float32),
        jnp.zeros((local_heads, row_count), jnp.float32),
        jnp.zeros((local_heads, row_count, HEAD), jnp.float32),
    )
    shard_rows = lax.all_gather(key_value, "ep", axis=0, tiled=True)
    piece_len = shard_rows.shape[0]
    key_span = 512

    def one_span(state_in, span_index):
        span_start = span_index * key_span

        def update(state_old):
            running_max, denominator, weighted = state_old
            block = lax.dynamic_slice_in_dim(shard_rows, span_index * key_span, key_span, 0)
            keys_block = block[:, :width].reshape(key_span, local_heads, HEAD)
            values_block = block[:, width:].reshape(key_span, local_heads, HEAD)
            key_gate = lax.dynamic_slice_in_dim(cum_gate, span_start, key_span, 1)
            scores = (
                jnp.einsum(
                    "qhd,khd->hqk", query_heads, keys_block, preferred_element_type=jnp.float32
                )
                * scale
            )
            scores = scores + query_gate[:, :, None] - key_gate[:, None, :]
            causal = (span_start + jnp.arange(key_span, dtype=jnp.int32))[None, :] <= query_pos[
                :, None
            ]
            scores = jnp.where(causal[None], scores, neg_fill)
            new_max = jnp.maximum(running_max, jnp.max(scores, axis=2))
            expon = jnp.where(causal[None], jnp.exp(scores - new_max[:, :, None]), 0.0)
            rescale = jnp.exp(running_max - new_max)
            denominator = denominator * rescale + jnp.sum(expon, axis=2)
            weighted = weighted * rescale[:, :, None] + jnp.einsum(
                "hqk,khd->hqd",
                expon.astype(jnp.bfloat16),
                values_block,
                preferred_element_type=jnp.float32,
            )
            return (new_max, denominator, weighted)

        state_next = lax.cond(span_start <= last_row, update, lambda unchanged: unchanged, state_in)
        return (state_next, None)

    state_out, _ = lax.scan(one_span, initial, jnp.arange(piece_len // key_span, dtype=jnp.int32))
    running_max, denominator, weighted = state_out
    heads_out = (weighted / denominator[:, :, None]).transpose(1, 0, 2).reshape(row_count, width)
    heads_out = heads_out.astype(jnp.bfloat16)
    token_count = moe_input.shape[0]
    top_count = routes.shape[1]
    local_experts = expert_gate.shape[0]
    ep_count = lax.axis_size("ep")
    expert_count = local_experts * ep_count
    capacity = 2 * token_count * top_count // expert_count
    column_count = expert_down.shape[2]
    first_column = lax.axis_index("tp") * column_count
    moe_rows = moe_input.astype(jnp.float32)
    normed = (
        moe_rows
        * lax.rsqrt(jnp.mean(moe_rows * moe_rows, axis=1, keepdims=True) + norm_eps)
        * moe_gain
    ).astype(jnp.bfloat16)
    flat_routes = routes.reshape(-1)
    one_hot = (flat_routes[:, None] == jnp.arange(expert_count, dtype=jnp.int32)[None, :]).astype(
        jnp.int32
    )
    ranks = jnp.sum(jnp.cumsum(one_hot, axis=0) * one_hot, axis=1) - 1
    slot_index = flat_routes * capacity + ranks
    pair_token = jnp.arange(token_count * top_count, dtype=jnp.int32) // top_count
    slot_token = (
        jnp.full((expert_count * capacity,), token_count, jnp.int32).at[slot_index].set(pair_token)
    )
    padded = jnp.concatenate([normed, jnp.zeros((1, normed.shape[1]), jnp.bfloat16)], axis=0)
    outgoing = lax.dynamic_slice_in_dim(padded, first_column, column_count, 1)[slot_token]
    outgoing = outgoing.reshape(ep_count, local_experts, capacity, outgoing.shape[1])
    arrived = lax.all_to_all(outgoing, "ep", split_axis=0, concat_axis=0, tiled=True)
    arrived = lax.all_gather(arrived, "tp", axis=3, tiled=True)
    gate_val = jnp.einsum(
        "aecd,edf->aecf", arrived, expert_gate, preferred_element_type=jnp.float32
    )
    up_val = jnp.einsum("aecd,edf->aecf", arrived, expert_up, preferred_element_type=jnp.float32)
    hidden = (jax.nn.silu(gate_val) * up_val).astype(jnp.bfloat16)
    hidden = lax.all_gather(hidden, "tp", axis=3, tiled=True)
    result = jnp.einsum(
        "aecf,efd->aecd", hidden, expert_down, preferred_element_type=jnp.float32
    ).astype(jnp.bfloat16)
    returned = lax.all_to_all(result, "ep", split_axis=0, concat_axis=0, tiled=True)
    picked = returned.reshape(expert_count * capacity, column_count)[slot_index]
    picked = picked.astype(jnp.float32).reshape(token_count, top_count, column_count)
    routed = jnp.sum(picked * route_weight[:, :, None], axis=1)
    shared_hidden = (
        jax.nn.silu(jnp.dot(normed, shared_gate, preferred_element_type=jnp.float32))
        * jnp.dot(normed, shared_up, preferred_element_type=jnp.float32)
    ).astype(jnp.bfloat16)
    heads_all, shared_all = (
        lax.all_gather(heads_out, "tp", axis=1, tiled=True),
        lax.all_gather(shared_hidden, "tp", axis=1, tiled=True),
    )
    mixer_sum = jnp.dot(heads_all, out_weight, preferred_element_type=jnp.float32)
    moe_total = routed + jnp.dot(shared_all, shared_down, preferred_element_type=jnp.float32)
    return (mixer_sum.astype(jnp.bfloat16), moe_total.astype(jnp.bfloat16))


def solution(mesh):
    placed = (
        P("ep", "tp"),
        P("ep", "tp"),
        P("ep", "tp"),
        P("tp", None),
        P(None, "tp"),
        P("ep", None),
        P(),
        P("ep", None),
        P("ep", None),
        P("ep", None, "tp"),
        P("ep", None, "tp"),
        P("ep", None, "tp"),
        P(None, "tp"),
        P(None, "tp"),
        P(None, "tp"),
    )
    return jax.shard_map(
        local, mesh=mesh, in_specs=placed, out_specs=(P("ep", "tp"), P("ep", "tp")), check_vma=False
    )
```

profile of v0, /device:TPU:0, one launch (start us, length us, event | category | flops | bytes accessed | tf_op | source)
XLA Modules:
  0.0 447.6 jit_solution(2679872729784148897)
XLA Ops:
  12.8 4.1 scatter_custom_fusion
  18.3 4.7 %gather_fusion = bf16[1152,512]{1,0:T(8,128)(2,1)} fusion(bf16[193,512]{1,0:T(8,128)(2,1)S(1)} %pad_dynamic-slice_fusion, s32[2048]{0:T(1024)S(1)} %pad_clamp_fusion), kind=kCustom, calls=%fused_computation | custom fusion | bytes 2363904 | tf_op jit(solution)/shard_map/gather | solution.py:111
  23.0 2.9 reshape.119
  27.9 35.5 %all_to_all.10 = bf16[8,4,36,512]{3,1,2,0:T(4,128)(2,1)S(1)} all-to-all(bf16[8,4,36,512]{3,1,2,0:T(4,128)(2,1)S(1)} %copy.41), channel_id=1, replica_groups=mesh['ep'=8,'tp'=4] {'ep'}, dimensions={0} | all-to-all | bytes 2359296 | tf_op jit(solution)/shard_map/all_to_all | solution.py:113
  64.8 60.2 %all-gather.9.cloned.1.call-done = bf16[8,4,36,2048]{3,2,0,1:T(8,128)(2,1)} async-done(((bf16[8,4,36,512]{3,2,0,1:T(8,128)(2,1)}), bf16[8,4,36,2048]{3,2,0,1:T(8,128)(2,1)}) %all-gather.9.cloned.1.call-update) | async-done | bytes 4718608 | tf_op jit(solution)/shard_map/all_gather | solution.py:114
  125.0 4.8 %fusion.29 = f32[8,4,36,128]{3,2,0,1:T(8,128)S(1)} fusion(bf16[8,4,36,2048]{3,2,0,1:T(8,128)(2,1)} %all-gather.9.cloned.1.call-done, bf16[4,2048,128]{2,1,0:T(8,128)(2,1)} %param.28), kind=kOutput, calls=%fused_computation.37 | convolution fusion | flops 603979776 | bytes 7405568 | tf_op jit(solution)/shard_map/aecd,edf->aecf/dot_general | solution.py:115
  140.4 21.0 %all-gather.11.cloned.1.call-done = bf16[8,4,36,512]{3,2,0,1:T(8,128)(2,1)} async-done(((bf16[8,4,36,128]{3,2,0,1:T(8,128)(2,1)}), bf16[8,4,36,512]{3,2,0,1:T(8,128)(2,1)}) %all-gather.11.cloned.1.call-update) | async-done | bytes 1179664 | tf_op jit(solution)/shard_map/all_gather | solution.py:120
  165.5 4.6 %all-to-all-start.1 = ((bf16[8,4,36,512]{3,1,2,0:T(4,128)(2,1)}), bf16[8,4,36,512]{3,1,2,0:T(4,128)(2,1)}, u32[]{:S(2)}, u32[]{:S(2)}) async-start(bf16[8,4,36,512]{3,1,2,0:T(4,128)(2,1)} %copy.43), calls=%async_computation.1 | async-start | bytes 2359296 | tf_op jit(solution)/shard_map/all_to_all | solution.py:124
  170.3 81.3 %all-gather.5.cloned.1.call-done = bf16[6144,512]{0,1:T(8,128)(2,1)} async-done(((bf16[768,512]{0,1:T(8,128)(2,1)}), bf16[6144,512]{0,1:T(8,128)(2,1)}) %all-gather.5.cloned.1.call-update) | async-done | bytes 6291472 | tf_op jit(solution)/shard_map/all_gather | solution.py:43
  252.6 39.0 %while.15 = (s32[]{:T(128)}, f32[4,768]{1,0:T(4,128)S(1)}, f32[4,768]{1,0:T(4,128)S(1)}, f32[4,768,64]{1,2,0:T(8,128)}, s32[12]{0:T(128)S(1)}, /*index=5*/s32[]{...) while((s32[]{:T(128)}, f32[4,768]{1,0:T(4,128)S(1)}, ...), condition=%wide.region_5.6_spmd.clone, body=%wide.region_0.5_spmd.clone.sunk | while | flops 433331456 | bytes 30568932 | solution.py:82
  253.9 11.5 %conditional.3 = ((f32[4,768]{1,0:T(4,128)S(1)}, f32[4,768]{1,0:T(4,128)S(1)}, f32[4,768,64]{1,2,0:T(8,128)})) conditional(s32[]{:T(128)} %convert_element_type.85, (f32[4,768]{1,0:T(4,128)S(1)}, f32[4,768]{1,0:T(4,128)S(1)}, f32[4,768,64]{1,2,0:T(8,128)}) %tuple.39, (s32[]{:T(128)}, s32[]{:T(128)}, s32[]{:T(128)}, bf16[6144,512]{0,1:T(8,128)(2,1)}, ...), branch_computations={%region_1.1_spmd, %region_2.4_spmd} | conditional | flops 433331456 | bytes 30565576 | solution.py:79
  256.7 2.9 fusion.4
  259.6 2.3 fusion.3
  262.0 2.5 fusion.8
  266.7 11.5 %conditional.3 = ((f32[4,768]{1,0:T(4,128)S(1)}, f32[4,768]{1,0:T(4,128)S(1)}, f32[4,768,64]{1,2,0:T(8,128)})) conditional(s32[]{:T(128)} %convert_element_type.85, (f32[4,768]{1,0:T(4,128)S(1)}, f32[4,768]{1,0:T(4,128)S(1)}, f32[4,768,64]{1,2,0:T(8,128)}) %tuple.39, (s32[]{:T(128)}, s32[]{:T(128)}, s32[]{:T(128)}, bf16[6144,512]{0,1:T(8,128)(2,1)}, ...), branch_computations={%region_1.1_spmd, %region_2.4_spmd} | conditional | flops 433331456 | bytes 30565576 | solution.py:79
  269.5 2.9 fusion.4
  274.8 2.5 fusion.8
  297.2 8.7 %all_gather.19 = bf16[192,512]{1,0:T(8,128)(2,1)S(1)} all-gather(bf16[192,128]{1,0:T(8,128)(2,1)S(1)} %fusion.42), channel_id=1, replica_groups=mesh['ep'=8,'tp'=4] {'tp'}, dimensions={1}, use_global_device_ids=true | all-gather | bytes 245760 | tf_op jit(solution)/shard_map/all_gather | solution.py:134
  305.9 2.6 copy.44
  310.7 3.3 gather_fusion.1
  313.9 2.5 reshape.122
  316.4 2.4 multiply_reduce_fusion
  319.8 117.7 %all-gather.7.cloned.1.call-done = bf16[768,1024]{0,1:T(8,128)(2,1)} async-done(((bf16[768,256]{0,1:T(8,128)(2,1)}), bf16[768,1024]{0,1:T(8,128)(2,1)}) %all-gather.7.cloned.1.call-update) | async-done | bytes 1572880 | tf_op jit(solution)/shard_map/all_gather | solution.py:133
  437.5 3.6 convolution_convert_fusion
  (122 shorter events, 51.0 us)
Async XLA Ops:
  7.2 154.2 %copy-start = (bf16[4,512,512]{2,1,0:T(8,128)(2,1)S(1)}, bf16[4,512,512]{2,1,0:T(8,128)(2,1)}, u32[]{:S(2)}) copy-start(bf16[4,512,512]{2,1,0:T(8,128)(2,1)} %param.30) | copy-start | bytes 6291460
  7.2 117.9 %all-gather.9.cloned.1.call-start = ((), (), s32[]{:S(2)}) async-start(), calls=%async_computation.4 | async-start | bytes 6553600 | tf_op jit(solution)/shard_map/all_gather | solution.py:114
  64.8 96.6 %all-gather.11.cloned.1.call-start = ((), (), s32[]{:S(2)}) async-start(), calls=%async_computation.5 | async-start | bytes 1638400 | tf_op jit(solution)/shard_map/all_gather | solution.py:120
  125.0 4.8 %copy-start.1 = (bf16[8,4,36,2048]{3,2,0,1:T(8,128)(2,1)S(1)}, bf16[8,4,36,2048]{3,2,0,1:T(8,128)(2,1)}, u32[]{:S(2)}) copy-start(bf16[8,4,36,2048]{3,2,0,1:T(8,128)(2,1)} %all-gather.9.cloned.1.call-done) | copy-start | bytes 14155780
  125.0 5.3 %copy-start.7 = (bf16[4,2048,128]{2,1,0:T(8,128)(2,1)S(1)}, bf16[4,2048,128]{2,1,0:T(8,128)(2,1)}, u32[]{:S(2)}) copy-start(bf16[4,2048,128]{2,1,0:T(8,128)(2,1)} %param.29) | copy-start | bytes 6291460
  132.6 119.0 %all-gather.5.cloned.1.call-start = ((), (), s32[]{:S(2)}) async-start(), calls=%async_computation.2 | async-start | bytes 7077888 | tf_op jit(solution)/shard_map/all_gather | solution.py:43
  165.5 140.4 %all-to-all-start.1 = ((bf16[8,4,36,512]{3,1,2,0:T(4,128)(2,1)}), bf16[8,4,36,512]{3,1,2,0:T(4,128)(2,1)}, u32[]{:S(2)}, u32[]{:S(2)}) async-start(bf16[8,4,36,512]{3,1,2,0:T(4,128)(2,1)} %copy.43), calls=%async_computation.1 | async-start | bytes 2359296 | tf_op jit(solution)/shard_map/all_to_all | solution.py:124
  170.1 267.4 %all-gather.7.cloned.1.call-start = ((), (), s32[]{:S(2)}) async-start(), calls=%async_computation.3 | async-start | bytes 1966080 | tf_op jit(solution)/shard_map/all_gather | solution.py:133
  252.6 41.0 %copy-start.6 = (f32[192,3]{0,1:T(4,128)S(1)}, f32[192,3]{0,1:T(4,128)}, u32[]{:S(2)}) copy-start(f32[192,3]{0,1:T(4,128)} %param.27) | copy-start | bytes 6916
  259.6 2.4 copy-start.2
  264.5 0.9 copy-start.3
  272.4 2.4 copy-start.2
  277.3 0.9 copy-start.3
  313.9 2.5 copy-start.5
  313.9 5.0 %copy-start.4 = (bf16[512,512]{1,0:T(8,128)(2,1)S(1)}, bf16[512,512]{1,0:T(8,128)(2,1)}, u32[]{:S(2)}) copy-start(bf16[512,512]{1,0:T(8,128)(2,1)} %param.33) | copy-start | bytes 1572868
Sparse Core Ops, SparseCore 0:
  64.9 60.0 all-gather.8
  132.8 28.5 all-gather.10
  163.5 88.0 all-gather.4
  293.7 143.7 all-gather.6
where the time goes:
time: 450 us; the launch traced here: 448 us
  waiting for transfers between devices  280 us (62%)
  local copies, waits for them, and re-layouts  50.3 us (11%)
  blocking collectives  44.2 us (10%)
  matrix products  27.4 us (6%)
  other arithmetic  16.8 us (4%)
  between operations  14 us (3%)
  loops' own time  9.67 us (2%)
  starting transfers between devices  4.94 us (1%)
    all_gather x1, waiting for transfers between devices, local(): lax.all_gather(heads_out, 'tp', axis=1, tiled=True)  118 us
    all_gather x1, waiting for transfers between devices, local(): shard_rows = lax.all_gather(key_value, 'ep', axis=0, tiled=True)  81.3 us
    all_gather x1, waiting for transfers between devices, local(): arrived = lax.all_gather(arrived, 'tp', axis=3, tiled=True)  60.2 us
    all_to_all x1, blocking collectives, local(): lax.all_to_all(outgoing, 'ep', split_axis=0, concat_axis=0, tiled=True)  35.5 us
    all_gather x1, waiting for transfers between devices, local(): hidden = lax.all_gather(hidden, 'tp', axis=3, tiled=True)  21 us
  transfers between devices with their start and end apart: 5, of which 4 were waited for; matrix products, arithmetic and copies ran while one was open for 13% of the time, Pallas kernels for 0%

commit v1 on v0

--- a/solution.py
+++ b/solution.py
@@ -40,7 +40,12 @@
         jnp.zeros((local_heads, row_count), jnp.float32),
         jnp.zeros((local_heads, row_count, HEAD), jnp.float32),
     )
-    shard_rows = lax.all_gather(key_value, "ep", axis=0, tiled=True)
+    ring = [key_value]
+    for hop in range(7):
+        ring.append(lax.ppermute(ring[-1], "ep", [(dev, (dev + 1) % 8) for dev in range(8)]))
+    shard_rows = jnp.roll(
+        jnp.concatenate(ring[::-1], axis=0), (lax.axis_index("ep") + 1) * ring[0].shape[0], axis=0
+    )
     piece_len = shard_rows.shape[0]
     key_span = 512
 

time: 450 us -> 412 us (0.916)
  waiting for transfers between devices: 280 us -> 104 us
  starting transfers between devices: 4.94 us -> 105 us
  local copies, waits for them, and re-layouts: 50.3 us -> 89.2 us
    all_gather x1, waiting for transfers between devices: 118 us -> 10.9 us  [local(): lax.all_gather(heads_out, 'tp', axis=1, tiled=True)]
    all_to_all x1, starting transfers between devices: 4.6 us -> 105 us  [local(): lax.all_to_all(result, 'ep', split_axis=0, concat_axis=0, tiled=True)]
    ppermute x0 -> x7, waiting for transfers between devices: none -> 90.1 us  [local(): lax.ppermute(ring[-1], 'ep', [(dev, (dev + 1) % 8) for dev in range(8)])]
    all_gather x1 -> x0, waiting for transfers between devices: 81.3 us -> none  [local(): shard_rows = lax.all_gather(key_value, 'ep', axis=0, tiled=True)]
    all_gather x1, waiting for transfers between devices: 60.2 us -> 0.01 us  [local(): arrived = lax.all_gather(arrived, 'tp', axis=3, tiled=True)]
    unnamed x17 -> x51, local copies, waits for them, and re-layouts: 7.06 us -> 37.1 us
    all_gather x1, waiting for transfers between devices: 21 us -> 0.02 us  [local(): hidden = lax.all_gather(hidden, 'tp', axis=3, tiled=True)]
    dynamic_slice x0 -> x1, local copies, waits for them, and re-layouts: none -> 9.54 us  [local(): jnp.roll(jnp.concatenate(ring[::-1], axis=0), (lax.axis_index('ep') + 1)...]
  transfers between devices with their start and end apart: 5 -> 11, of which waited for: 4 -> 9; matrix products, arithmetic and copies ran while one was open for 13% -> 20% of each run, Pallas kernels for 0% -> 0%
where the time goes in v1:
time: 412 us; the launch traced here: 410 us
  starting transfers between devices  105 us (25%)
  waiting for transfers between devices  104 us (25%)
  local copies, waits for them, and re-layouts  89.2 us (22%)
  blocking collectives  44.3 us (11%)
  matrix products  26.6 us (6%)
  other arithmetic  17.8 us (4%)
  between operations  14 us (3%)
  loops' own time  8.71 us (2%)
    all_to_all x1, starting transfers between devices, local(): lax.all_to_all(result, 'ep', split_axis=0, concat_axis=0, tiled=True)  105 us
    ppermute x7, waiting for transfers between devices, local(): lax.ppermute(ring[-1], 'ep', [(dev, (dev + 1) % 8) for dev in range(8)])  90.1 us
    unnamed x51, local copies, waits for them, and re-layouts  37.1 us
    all_to_all x1, blocking collectives, local(): lax.all_to_all(outgoing, 'ep', split_axis=0, concat_axis=0, tiled=True)  35.5 us
    all_gather x1, waiting for transfers between devices, local(): lax.all_gather(heads_out, 'tp', axis=1, tiled=True)  10.9 us
    dynamic_slice x1, local copies, waits for them, and re-layouts, local(): jnp.roll(jnp.concatenate(ring[::-1], axis=0), (lax.axis_index('ep') + 1)...  9.54 us
    all_gather x1, blocking collectives, local(): lax.all_gather(shared_hidden, 'tp', axis=1, tiled=True)  8.74 us
  transfers between devices with their start and end apart: 11, of which 9 were waited for; matrix products, arithmetic and copies ran while one was open for 20% of the time, Pallas kernels for 0%

profile of v1, /device:TPU:0, one launch (start us, length us, event | category | flops | bytes accessed | tf_op | source)
XLA Modules:
  0.0 409.6 jit_solution(5757200894351019977)
XLA Ops:
  12.8 4.1 %scatter_custom_fusion = s32[1152]{0:T(1024)S(1)} fusion(s32[576]{0:T(1024)S(1)} %fusion.49, s32[576]{0:T(1024)S(1)} %add_select_fusion, s32[]{:T(128)} %constant.98.clone.1), kind=kCustom, calls=%fused_computation.83 | custom fusion | bytes 4612 | tf_op jit(solution)/shard_map/scatter | solution.py:113
  18.3 4.7 %gather_fusion = bf16[1152,512]{1,0:T(8,128)(2,1)} fusion(bf16[193,512]{1,0:T(8,128)(2,1)S(1)} %pad_dynamic-slice_fusion, s32[2048]{0:T(1024)S(1)} %pad_clamp_fusion), kind=kCustom, calls=%fused_computation | custom fusion | bytes 2363904 | tf_op jit(solution)/shard_map/gather | solution.py:116
  23.0 3.0 reshape.119
  27.9 35.5 %all_to_all.10 = bf16[8,4,36,512]{3,1,2,0:T(4,128)(2,1)S(1)} all-to-all(bf16[8,4,36,512]{3,1,2,0:T(4,128)(2,1)S(1)} %copy.41), channel_id=1, replica_groups=mesh['ep'=8,'tp'=4] {'ep'}, dimensions={0} | all-to-all | bytes 2359296 | tf_op jit(solution)/shard_map/all_to_all | solution.py:118
  69.0 13.2 %collective-permute-done = bf16[768,512]{0,1:T(8,128)(2,1)S(1)} collective-permute-done((bf16[768,512]{0,1:T(8,128)(2,1)S(1)}, bf16[768,512]{0,1:T(8,128)(2,1)S(1)}, u32[]{:S(2)}, u32[]{:S(2)}) %collective-permute-start) | collective-permute-done | bytes 786464 | tf_op jit(solution)/shard_map/ppermute | solution.py:45
  83.1 13.2 %collective-permute-done.1 = bf16[768,512]{0,1:T(8,128)(2,1)S(1)} collective-permute-done((bf16[768,512]{0,1:T(8,128)(2,1)S(1)}, bf16[768,512]{0,1:T(8,128)(2,1)S(1)}, u32[]{:S(2)}, u32[]{:S(2)}) %collective-permute-start.1) | collective-permute-done | bytes 786464 | tf_op jit(solution)/shard_map/ppermute | solution.py:45
  97.2 13.2 %collective-permute-done.2 = bf16[768,512]{0,1:T(8,128)(2,1)S(1)} collective-permute-done((bf16[768,512]{0,1:T(8,128)(2,1)S(1)}, bf16[768,512]{0,1:T(8,128)(2,1)S(1)}, u32[]{:S(2)}, u32[]{:S(2)}) %collective-permute-start.2) | collective-permute-done | bytes 786464 | tf_op jit(solution)/shard_map/ppermute | solution.py:45
  111.3 13.2 %collective-permute-done.3 = bf16[768,512]{0,1:T(8,128)(2,1)S(1)} collective-permute-done((bf16[768,512]{0,1:T(8,128)(2,1)S(1)}, bf16[768,512]{0,1:T(8,128)(2,1)S(1)}, u32[]{:S(2)}, u32[]{:S(2)}) %collective-permute-start.3) | collective-permute-done | bytes 786464 | tf_op jit(solution)/shard_map/ppermute | solution.py:45
  125.5 13.2 %collective-permute-done.4 = bf16[768,512]{0,1:T(8,128)(2,1)S(1)} collective-permute-done((bf16[768,512]{0,1:T(8,128)(2,1)S(1)}, bf16[768,512]{0,1:T(8,128)(2,1)S(1)}, u32[]{:S(2)}, u32[]{:S(2)}) %collective-permute-start.4) | collective-permute-done | bytes 786464 | tf_op jit(solution)/shard_map/ppermute | solution.py:45
  139.5 13.3 %collective-permute-done.5 = bf16[768,512]{0,1:T(8,128)(2,1)} collective-permute-done((bf16[768,512]{0,1:T(8,128)(2,1)S(1)}, bf16[768,512]{0,1:T(8,128)(2,1)}, u32[]{:S(2)}, u32[]{:S(2)}) %collective-permute-start.5) | collective-permute-done | bytes 786464 | tf_op jit(solution)/shard_map/ppermute | solution.py:45
  155.7 10.7 %collective-permute-done.6 = bf16[768,512]{0,1:T(8,128)(2,1)} collective-permute-done((bf16[768,512]{0,1:T(8,128)(2,1)}, bf16[768,512]{0,1:T(8,128)(2,1)}, u32[]{:S(2)}, u32[]{:S(2)}) %collective-permute-start.6) | collective-permute-done | bytes 786464 | tf_op jit(solution)/shard_map/ppermute | solution.py:45
  183.2 4.8 %fusion.29 = f32[8,4,36,128]{3,2,0,1:T(8,128)S(1)} fusion(bf16[8,4,36,2048]{3,2,0,1:T(8,128)(2,1)} %all-gather.6.cloned.1.call-done, bf16[4,2048,128]{2,1,0:T(8,128)(2,1)} %param.28), kind=kOutput, calls=%fused_computation.37 | convolution fusion | flops 603979776 | bytes 7405568 | tf_op jit(solution)/shard_map/aecd,edf->aecf/dot_general | solution.py:120
  201.7 9.5 %constant_dynamic-slice_fusion.3 = bf16[6144,512]{0,1:T(8,128)(2,1)} fusion(bf16[12288,512]{0,1:T(8,128)(2,1)} %constant_dynamic-update-slice_fusion, s32[]{:T(128)S(6)} %select_n.52), kind=kLoop, calls=%fused_computation.91 | loop fusion | bytes 12582916 | tf_op jit(solution)/shard_map/jit(_roll_dynamic)/dynamic_slice | solution.py:46
  212.2 35.4 %while.15 = (s32[]{:T(128)}, f32[4,768]{1,0:T(4,128)S(1)}, f32[4,768]{1,0:T(4,128)S(1)}, f32[4,768,64]{1,2,0:T(8,128)}, s32[12]{0:T(128)S(1)}, /*index=5*/s32[]{...) while((s32[]{:T(128)}, f32[4,768]{1,0:T(4,128)S(1)}, ...), condition=%wide.region_5.6_spmd.clone, body=%wide.region_0.5_spmd.clone.sunk | while | flops 433331456 | bytes 30568924 | solution.py:87
  213.3 10.5 %conditional.3 = ((f32[4,768]{1,0:T(4,128)S(1)}, f32[4,768]{1,0:T(4,128)S(1)}, f32[4,768,64]{1,2,0:T(8,128)})) conditional(s32[]{:T(128)} %convert_element_type.85, (f32[4,768]{1,0:T(4,128)S(1)}, f32[4,768]{1,0:T(4,128)S(1)}, f32[4,768,64]{1,2,0:T(8,128)}) %tuple.39, (s32[]{:T(128)}, s32[]{:T(128)}, s32[]{:T(128)}, bf16[6144,512]{0,1:T(8,128)(2,1)}, ...), branch_computations={%region_1.1_spmd, %region_2.4_spmd} | conditional | flops 433331456 | bytes 30565576 | solution.py:84
  225.0 10.5 %conditional.3 = ((f32[4,768]{1,0:T(4,128)S(1)}, f32[4,768]{1,0:T(4,128)S(1)}, f32[4,768,64]{1,2,0:T(8,128)})) conditional(s32[]{:T(128)} %convert_element_type.85, (f32[4,768]{1,0:T(4,128)S(1)}, f32[4,768]{1,0:T(4,128)S(1)}, f32[4,768,64]{1,2,0:T(8,128)}) %tuple.39, (s32[]{:T(128)}, s32[]{:T(128)}, s32[]{:T(128)}, bf16[6144,512]{0,1:T(8,128)(2,1)}, ...), branch_computations={%region_1.1_spmd, %region_2.4_spmd} | conditional | flops 433331456 | bytes 30565576 | solution.py:84
  232.1 2.5 fusion.8
  253.7 104.9 %all-to-all-start.1 = ((bf16[8,4,36,512]{3,1,2,0:T(4,128)(2,1)}), bf16[8,4,36,512]{3,1,2,0:T(4,128)(2,1)}, u32[]{:S(2)}, u32[]{:S(2)}) async-start(bf16[8,4,36,512]{3,1,2,0:T(4,128)(2,1)} %copy.43), calls=%async_computation.1 | async-start | bytes 2359296 | tf_op jit(solution)/shard_map/all_to_all | solution.py:129
  362.2 8.7 %all_gather.15 = bf16[192,512]{1,0:T(8,128)(2,1)S(1)} all-gather(bf16[192,128]{1,0:T(8,128)(2,1)S(1)} %fusion.42), channel_id=1, replica_groups=mesh['ep'=8,'tp'=4] {'tp'}, dimensions={1}, use_global_device_ids=true | all-gather | bytes 245760 | tf_op jit(solution)/shard_map/all_gather | solution.py:139
  371.0 10.9 %all-gather.4.cloned.1.call-done = bf16[768,1024]{0,1:T(8,128)(2,1)} async-done(((bf16[768,256]{0,1:T(8,128)(2,1)}), bf16[768,1024]{0,1:T(8,128)(2,1)}) %all-gather.4.cloned.1.call-update) | async-done | bytes 1572880 | tf_op jit(solution)/shard_map/all_gather | solution.py:138
  381.9 3.6 convolution_convert_fusion
  385.5 2.6 all-to-all-done.1
  388.1 2.6 copy.44
  392.9 3.3 gather_fusion.1
  (170 shorter events, 96.1 us)
Async XLA Ops:
  7.2 242.4 %copy-start = (bf16[4,512,512]{2,1,0:T(8,128)(2,1)S(1)}, bf16[4,512,512]{2,1,0:T(8,128)(2,1)}, u32[]{:S(2)}) copy-start(bf16[4,512,512]{2,1,0:T(8,128)(2,1)} %param.30) | copy-start | bytes 6291460
  7.2 176.0 %all-gather.6.cloned.1.call-start = ((), (), s32[]{:S(2)}) async-start(), calls=%async_computation.3 | async-start | bytes 6553600 | tf_op jit(solution)/shard_map/all_gather | solution.py:119
  64.8 184.8 %all-gather.8.cloned.1.call-start = ((), (), s32[]{:S(2)}) async-start(), calls=%async_computation.4 | async-start | bytes 1638400 | tf_op jit(solution)/shard_map/all_gather | solution.py:125
  68.9 13.3 %collective-permute-start = (bf16[768,512]{0,1:T(8,128)(2,1)S(1)}, bf16[768,512]{0,1:T(8,128)(2,1)S(1)}, u32[]{:S(2)}, u32[]{:S(2)}) collective-permute-start(bf16[768,512]{0,1:T(8,128)(2,1)S(1)} %pad_maximum_fusion), channel_id=1, source_target_pairs={{0,4},{4,8},{8,12},{12,16},{16,20},{20,24},{24,28},{28,0},{1,5},{5... | collective-permute-start | bytes 2359304 | tf_op jit(solution)/shard_map/ppermute | solution.py:45
  83.1 13.2 %collective-permute-start.1 = (bf16[768,512]{0,1:T(8,128)(2,1)S(1)}, bf16[768,512]{0,1:T(8,128)(2,1)S(1)}, u32[]{:S(2)}, u32[]{:S(2)}) collective-permute-start(bf16[768,512]{0,1:T(8,128)(2,1)S(1)} %collective-permute-done), channel_id=1, source_target_pairs={{0,4},{4,8},{8,12},{12,16},{16,20},{20,24},{24,28},{28,0},{1,5},{5... | collective-permute-start | bytes 2359304 | tf_op jit(solution)/shard_map/ppermute | solution.py:45
  97.2 13.2 %collective-permute-start.2 = (bf16[768,512]{0,1:T(8,128)(2,1)S(1)}, bf16[768,512]{0,1:T(8,128)(2,1)S(1)}, u32[]{:S(2)}, u32[]{:S(2)}) collective-permute-start(bf16[768,512]{0,1:T(8,128)(2,1)S(1)} %collective-permute-done.1), channel_id=1, source_target_pairs={{0,4},{4,8},{8,12},{12,16},{16,20},{20,24},{24,28},{28,0},{1,5},{5... | collective-permute-start | bytes 2359304 | tf_op jit(solution)/shard_map/ppermute | solution.py:45
  111.3 13.2 %collective-permute-start.3 = (bf16[768,512]{0,1:T(8,128)(2,1)S(1)}, bf16[768,512]{0,1:T(8,128)(2,1)S(1)}, u32[]{:S(2)}, u32[]{:S(2)}) collective-permute-start(bf16[768,512]{0,1:T(8,128)(2,1)S(1)} %collective-permute-done.2), channel_id=1, source_target_pairs={{0,4},{4,8},{8,12},{12,16},{16,20},{20,24},{24,28},{28,0},{1,5},{5... | collective-permute-start | bytes 2359304 | tf_op jit(solution)/shard_map/ppermute | solution.py:45
  125.5 13.2 %collective-permute-start.4 = (bf16[768,512]{0,1:T(8,128)(2,1)S(1)}, bf16[768,512]{0,1:T(8,128)(2,1)S(1)}, u32[]{:S(2)}, u32[]{:S(2)}) collective-permute-start(bf16[768,512]{0,1:T(8,128)(2,1)S(1)} %collective-permute-done.3), channel_id=1, source_target_pairs={{0,4},{4,8},{8,12},{12,16},{16,20},{20,24},{24,28},{28,0},{1,5},{5... | collective-permute-start | bytes 2359304 | tf_op jit(solution)/shard_map/ppermute | solution.py:45
  139.5 13.3 %collective-permute-start.5 = (bf16[768,512]{0,1:T(8,128)(2,1)S(1)}, bf16[768,512]{0,1:T(8,128)(2,1)}, u32[]{:S(2)}, u32[]{:S(2)}) collective-permute-start(bf16[768,512]{0,1:T(8,128)(2,1)S(1)} %collective-permute-done.4), channel_id=1, source_target_pairs={{0,4},{4,8},{8,12},{12,16},{16,20},{20,24},{24,28},{28,0},{1,5},{5... | collective-permute-start | bytes 2359304 | tf_op jit(solution)/shard_map/ppermute | solution.py:45
  152.9 13.5 %collective-permute-start.6 = (bf16[768,512]{0,1:T(8,128)(2,1)}, bf16[768,512]{0,1:T(8,128)(2,1)}, u32[]{:S(2)}, u32[]{:S(2)}) collective-permute-start(bf16[768,512]{0,1:T(8,128)(2,1)} %collective-permute-done.5), channel_id=1, source_target_pairs={{0,4},{4,8},{8,12},{12,16},{16,20},{20,24},{24,28},{28,0},{1,5},{5... | collective-permute-start | bytes 2359304 | tf_op jit(solution)/shard_map/ppermute | solution.py:45
  154.8 20.0 %copy-start.10 = (bf16[768,512]{0,1:T(8,128)(2,1)S(1)}, bf16[768,512]{0,1:T(8,128)(2,1)}, u32[]{:S(2)}) copy-start(bf16[768,512]{0,1:T(8,128)(2,1)} %copy-done.9) | copy-start | bytes 2359300
  154.8 21.0 %copy-start.8 = (bf16[768,512]{0,1:T(8,128)(2,1)S(1)}, bf16[768,512]{0,1:T(8,128)(2,1)}, u32[]{:S(2)}) copy-start(bf16[768,512]{0,1:T(8,128)(2,1)} %copy-done.7) | copy-start | bytes 2359300
  154.8 22.0 %copy-start.5 = (bf16[768,512]{0,1:T(8,128)(2,1)S(1)}, bf16[768,512]{0,1:T(8,128)(2,1)}, u32[]{:S(2)}) copy-start(bf16[768,512]{0,1:T(8,128)(2,1)} %copy-done.4) | copy-start | bytes 2359300
  154.8 23.0 %copy-start.1 = (bf16[768,256]{0,1:T(8,128)(2,1)S(1)}, bf16[768,256]{0,1:T(8,128)(2,1)}, u32[]{:S(2)}) copy-start(bf16[768,256]{0,1:T(8,128)(2,1)} %copy.35) | copy-start | bytes 1179652
  183.2 4.8 %copy-start.3 = (bf16[8,4,36,2048]{3,2,0,1:T(8,128)(2,1)S(1)}, bf16[8,4,36,2048]{3,2,0,1:T(8,128)(2,1)}, u32[]{:S(2)}) copy-start(bf16[8,4,36,2048]{3,2,0,1:T(8,128)(2,1)} %all-gather.6.cloned.1.call-done) | copy-start | bytes 14155780
  183.2 5.3 %copy-start.17 = (bf16[4,2048,128]{2,1,0:T(8,128)(2,1)S(1)}, bf16[4,2048,128]{2,1,0:T(8,128)(2,1)}, u32[]{:S(2)}) copy-start(bf16[4,2048,128]{2,1,0:T(8,128)(2,1)} %param.29) | copy-start | bytes 6291460
  190.8 191.1 %all-gather.4.cloned.1.call-start = ((), (), s32[]{:S(2)}) async-start(), calls=%async_computation.2 | async-start | bytes 1966080 | tf_op jit(solution)/shard_map/all_gather | solution.py:138
  191.0 8.7 %copy-start.6 = (bf16[768,512]{0,1:T(8,128)(2,1)S(1)}, bf16[768,512]{0,1:T(8,128)(2,1)}, u32[]{:S(2)}) copy-start(bf16[768,512]{0,1:T(8,128)(2,1)} %copy-done.4) | copy-start | bytes 2359300
  191.0 9.6 %copy-start.2 = (bf16[768,256]{0,1:T(8,128)(2,1)S(1)}, bf16[768,256]{0,1:T(8,128)(2,1)}, u32[]{:S(2)}) copy-start(bf16[768,256]{0,1:T(8,128)(2,1)} %copy.35) | copy-start | bytes 1179652
  201.7 10.5 %copy-start.15 = (bf16[768,256]{0,1:T(8,128)(2,1)S(1)}, bf16[768,256]{0,1:T(8,128)(2,1)}, u32[]{:S(2)}) copy-start(bf16[768,256]{0,1:T(8,128)(2,1)} %copy.36) | copy-start | bytes 1179652
  216.1 4.3 %copy-start.13 = (f32[4,768,64]{1,2,0:T(8,128)S(1)}, f32[4,768,64]{1,2,0:T(8,128)}, u32[]{:S(2)}) copy-start(f32[4,768,64]{1,2,0:T(8,128)} %get-tuple-element.79) | copy-start | bytes 2359300 | tf_op jit(solution)/shard_map/while/body/eval_jaxpr/cond
  227.8 4.3 %copy-start.13 = (f32[4,768,64]{1,2,0:T(8,128)S(1)}, f32[4,768,64]{1,2,0:T(8,128)}, u32[]{:S(2)}) copy-start(f32[4,768,64]{1,2,0:T(8,128)} %get-tuple-element.79) | copy-start | bytes 2359300 | tf_op jit(solution)/shard_map/while/body/eval_jaxpr/cond
  247.6 111.1 %copy-start.16 = (f32[192,3]{0,1:T(4,128)S(1)}, f32[192,3]{0,1:T(4,128)}, u32[]{:S(2)}) copy-start(f32[192,3]{0,1:T(4,128)} %param.27) | copy-start | bytes 6916
  253.7 134.4 %all-to-all-start.1 = ((bf16[8,4,36,512]{3,1,2,0:T(4,128)(2,1)}), bf16[8,4,36,512]{3,1,2,0:T(4,128)(2,1)}, u32[]{:S(2)}, u32[]{:S(2)}) async-start(bf16[8,4,36,512]{3,1,2,0:T(4,128)(2,1)} %copy.43), calls=%async_computation.1 | async-start | bytes 2359296 | tf_op jit(solution)/shard_map/all_to_all | solution.py:129
  (7 other events, 6.2 us)
Sparse Core Ops, SparseCore 0:
  64.9 60.0 all-gather.5
  190.9 26.7 all-gather.7
  249.7 132.1 all-gather.3
